TPU v7x, 32 devices: a whole 2x2x4 slice. The times are simulated.
32 devices in a mesh: ep: 8 (over z, x), tp: 4 (over y, core).
Axes of the slice: x: 2, y: 2, z: 4, core: 2. Of those that a mesh axis runs over, the one named last changes fastest.
Arguments:
- queries: bfloat16 [2048, 1024], P('ep', 'tp'), may hold values from -256 to 256
- key_rows: bfloat16 [2048, 1024], P('ep', 'tp'), may hold values from -8 to 8
- value_rows: bfloat16 [2048, 1024], P('ep', 'tp'), may hold values from -6 to 6
- head_lambda: float32 [8], P('tp'), may hold values from 0.3 to 0.8
- sub_gain: float32 [128], replicated, may hold values from 0.1 to 1.9
- out_weight: bfloat16 [1024, 2048], P('tp'), may hold values from -0.1875 to 0.1875
- expert_input: bfloat16 [1536, 2048], P('ep'), may hold values from -6 to 6
- norm_gain: float32 [2048], replicated, may hold values from 0.1 to 1.9
- route_ids: int32 [1536, 2], P('ep'), may hold values from 0 to 7, all different within a row; in each aligned block of 192 rows (0 to 191, 192 to 383, ...) at most 80 rows name the same one
- route_weight: float32 [1536, 2], P('ep'), may hold values from 0.25 to 1
- gate_weight: bfloat16 [8, 2048, 3584], P('ep', None, 'tp'), may hold values from -0.125 to 0.125
- up_weight: bfloat16 [8, 2048, 3584], P('ep', None, 'tp'), may hold values from -0.125 to 0.125
- down_weight: bfloat16 [8, 3584, 2048], P('ep', 'tp'), may hold values from -0.09375 to 0.09375
Outputs:
- mixer_out: bfloat16 [2048, 2048], P(('ep', 'tp'))
- expert_out: bfloat16 [1536, 2048], P('ep', 'tp')
Inputs may be any that keep to these rules, and one draw needn't show every extreme that they name: `route_ids`: each row names 2 different experts. In each aligned block of 192 rows no expert is named by more than 80 rows, a bound that some block reaches.
All inputs are finite; a program needn't handle non-finite values.
Results may differ from a plain program's by a relative error of at most 0.014.
Values may be sent and summed in bfloat16 or wider, within the bound.
A program may use at most 256 MiB of HBM per device.

v0:
```python
import jax
import jax.numpy as jnp
from jax import lax
from jax.sharding import PartitionSpec as P

EPS = 1e-06


def mixer_half(queries, key_rows, value_rows, head_lambda, sub_gain, out_weight):
    rows_here = queries.shape[0]
    heads_here = head_lambda.shape[0]
    head_width = queries.shape[1] // (2 * heads_here)
    value_width = value_rows.shape[1] // heads_here
    scaling = head_width ** (-0.5)
    query_blocks = queries.reshape(rows_here, heads_here, 2, head_width)
    query_pos = lax.axis_index("ep") * rows_here + jnp.arange(rows_here, dtype=jnp.int32)
    row_max = jnp.full((heads_here, 2, rows_here), -1e30, jnp.float32)
    key_piece = lax.all_gather(key_rows, "ep", axis=0, tiled=True)
    value_piece = lax.all_gather(value_rows, "ep", axis=0, tiled=True)
    length = key_piece.shape[0]
    key_blocks = key_piece.reshape(length, heads_here, 2, head_width)
    value_blocks = value_piece.reshape(length, heads_here, value_width)
    scores = (
        jnp.einsum("qhmd,khmd->hmqk", query_blocks, key_blocks, preferred_element_type=jnp.float32)
        * scaling
    )
    allowed = query_pos[:, None] >= jnp.arange(length, dtype=jnp.int32)[None, :]
    scores = jnp.where(allowed, scores, -1e30)
    new_max = jnp.maximum(row_max, jnp.max(scores, axis=-1))
    weights = jnp.where(allowed, jnp.exp(scores - new_max[..., None]), 0.0)
    row_total = jnp.sum(weights, axis=-1)
    numerator = jnp.einsum(
        "hmqk,khd->hmqd",
        weights.astype(jnp.bfloat16),
        value_blocks,
        preferred_element_type=jnp.float32,
    )
    row_max, row_total, numerator = (new_max, row_total, numerator)
    per_map = numerator / row_total[..., None]
    contrast = per_map[:, 0] - head_lambda[:, None, None] * per_map[:, 1]
    normed = (
        contrast * lax.rsqrt(jnp.mean(contrast * contrast, axis=-1, keepdims=True) + EPS) * sub_gain
    ).astype(jnp.bfloat16)
    attended = jnp.transpose(normed, (1, 0, 2)).reshape(rows_here, heads_here * value_width)
    return lax.psum_scatter(
        jnp.dot(attended, out_weight, preferred_element_type=jnp.float32).astype(jnp.bfloat16),
        "tp",
        scatter_dimension=0,
        tiled=True,
    )


def expert_half(
    expert_input, norm_gain, route_ids, route_weight, gate_weight, up_weight, down_weight
):
    rows_here, model_width = expert_input.shape
    experts = lax.axis_size("ep")
    top_count = route_ids.shape[1]
    capacity = 5 * top_count * rows_here // (3 * experts)
    slots = experts * capacity
    wide_rows = expert_input.astype(jnp.float32)
    normed = (
        wide_rows
        * lax.rsqrt(jnp.mean(wide_rows * wide_rows, axis=-1, keepdims=True) + EPS)
        * norm_gain
    ).astype(jnp.bfloat16)
    flat_ids = route_ids.reshape(-1)
    onehot = (flat_ids[:, None] == jnp.arange(experts, dtype=jnp.int32)[None, :]).astype(jnp.int32)
    rank_before = jnp.cumsum(onehot, axis=0) - onehot
    slot_index = jnp.sum(rank_before * onehot, axis=1)
    buffer_pos = (flat_ids * capacity + slot_index).reshape(rows_here, top_count)
    matches = buffer_pos[None, :, :] == jnp.arange(slots, dtype=jnp.int32)[:, None, None]
    dispatch = jnp.any(matches, axis=-1).astype(jnp.bfloat16)
    combine = jnp.sum(jnp.where(matches, route_weight[None, :, :], 0.0), axis=-1)
    gate_mat = gate_weight[0]
    up_mat = up_weight[0]
    down_mat = down_weight[0]
    outgoing = jnp.dot(dispatch, normed, preferred_element_type=jnp.float32).astype(jnp.bfloat16)
    arrived = lax.all_to_all(
        outgoing.reshape(experts, capacity, model_width),
        "ep",
        split_axis=0,
        concat_axis=0,
        tiled=True,
    ).reshape(slots, model_width)
    gate_act = jnp.dot(arrived, gate_mat, preferred_element_type=jnp.float32)
    up_act = jnp.dot(arrived, up_mat, preferred_element_type=jnp.float32)
    hidden = (jax.nn.silu(gate_act) * up_act).astype(jnp.bfloat16)
    partial_result = jnp.dot(hidden, down_mat, preferred_element_type=jnp.float32)
    summed = lax.psum_scatter(
        partial_result.astype(jnp.bfloat16), "tp", scatter_dimension=1, tiled=True
    )
    col_count = summed.shape[1]
    returned = lax.all_to_all(
        summed.reshape(experts, capacity, col_count), "ep", split_axis=0, concat_axis=0, tiled=True
    ).reshape(slots, col_count)
    mixed = lax.dot_general(
        combine,
        returned.astype(jnp.float32),
        (((0,), (0,)), ((), ())),
        precision=lax.Precision.HIGHEST,
        preferred_element_type=jnp.float32,
    )
    return mixed.astype(jnp.bfloat16)


def shards(
    queries,
    key_rows,
    value_rows,
    head_lambda,
    sub_gain,
    out_weight,
    expert_input,
    norm_gain,
    route_ids,
    route_weight,
    gate_weight,
    up_weight,
    down_weight,
):
    mixer_out = mixer_half(queries, key_rows, value_rows, head_lambda, sub_gain, out_weight)
    expert_out = expert_half(
        expert_input, norm_gain, route_ids, route_weight, gate_weight, up_weight, down_weight
    )
    return (mixer_out, expert_out)


def solution(mesh):
    placed = (
        P("ep", "tp"),
        P("ep", "tp"),
        P("ep", "tp"),
        P("tp"),
        P(),
        P("tp", None),
        P("ep", None),
        P(),
        P("ep", None),
        P("ep", None),
        P("ep", None, "tp"),
        P("ep", None, "tp"),
        P("ep", "tp", None),
    )
    return jax.shard_map(
        shards,
        mesh=mesh,
        in_specs=placed,
        out_specs=(P(("ep", "tp"), None), P("ep", "tp")),
        check_vma=False,
    )
```

profile of v0, /device:TPU:0, one launch (start us, length us, event | category | flops | bytes accessed | tf_op | source)
XLA Modules:
  0.0 183.7 jit_solution(2173405152536160842)
XLA Ops:
  8.0 0.0 copy-start
  8.0 0.9 copy.43
  8.9 0.1 eq.42
  9.0 0.1 eq.38
  9.2 0.9 reduce-window.6
  10.1 0.2 slice_reduce_fusion
  10.3 0.1 fusion.32
  10.4 0.1 reduce_sum.50
  10.6 0.1 copy.45
  10.6 0.7 multiply_add_fusion
  11.3 0.1 fusion.23
  11.5 1.4 fusion.17
  12.9 3.6 %convolution_convert_fusion = bf16[640,2048]{1,0:T(8,128)(2,1)} fusion(pred[640,192]{0,1:T(8,128)(4,1)S(1)} %fusion.23, bf16[192,2048]{1,0:T(8,128)(2,1)} %param.19, f32[2048]{0:T(1024)} %param.20, f32[192]{0:T(256)S(1)} %add_rsqrt_fusion.1), kind=kOutput, calls=%fused_computation.14 | convolution fusion | flops 506200064 | bytes 3539712 | tf_op jit(solution)/shard_map/dot_general | solution.py:78
  16.5 7.3 %all-to-all-start = ((bf16[8,80,2048]{2,1,0:T(8,128)(2,1)}), bf16[8,80,2048]{2,1,0:T(8,128)(2,1)}, u32[]{:S(2)}, u32[]{:S(2)}) async-start(bf16[8,80,2048]{2,1,0:T(8,128)(2,1)} %bitcast.68), calls=%async_computation.1 | async-start | bytes 5242880 | tf_op jit(solution)/shard_map/all_to_all | solution.py:79
  23.8 0.0 all-gather.3.cloned.1.call-start
  23.8 0.7 all-gather.3.cloned.1.call-update
  24.5 0.0 all-gather.5.cloned.1.call-start
  24.6 0.7 all-gather.5.cloned.1.call-update
  25.3 0.0 reduce-scatter.5.cloned.1.call-start
  25.3 70.7 %all-to-all-done = bf16[8,80,2048]{2,1,0:T(8,128)(2,1)} async-done(((bf16[8,80,2048]{2,1,0:T(8,128)(2,1)}), bf16[8,80,2048]{2,1,0:T(8,128)(2,1)}, u32[]{:S(2)}, u32[]{:S(2)}) %all-to-all-start) | async-done | bytes 2621472 | tf_op jit(solution)/shard_map/all_to_all | solution.py:79
  96.0 7.2 %fusion.10 = f32[640,896]{1,0:T(8,128)} fusion(bf16[640,2048]{1,0:T(8,128)(2,1)} %bitcast.12, bf16[1,2048,896]{2,1,0:T(8,128)(2,1)} %param.23), kind=kOutput, calls=%fused_computation.11 | convolution fusion | flops 2348810240 | bytes 8585216 | tf_op jit(solution)/shard_map/dot_general | solution.py:86
  103.2 11.8 %fusion.12 = bf16[640,2048]{1,0:T(8,128)(2,1)} fusion(bf16[1,896,2048]{2,1,0:T(8,128)(2,1)} %param.25, f32[640,896]{1,0:T(8,128)} %fusion.10, bf16[640,2048]{1,0:T(8,128)(2,1)} %bitcast.12, bf16[1,2048,896]{2,1,0:T(8,128)(2,1)} %param.24), kind=kOutput, calls=%fused_computation.13 | convolution fusion | flops 4702371840 | bytes 14876672 | tf_op jit(solution)/shard_map/dot_general | solution.py:89
  115.0 0.0 reduce-scatter.5.cloned.1.call-update
  115.0 0.2 reduce-scatter.3.cloned.1.call-start
  115.3 0.1 copy.39
  115.4 0.4 iota_compare_fusion
  115.8 0.0 all-gather.3.cloned.1.call-done
  115.8 1.5 copy.40
  117.3 11.8 %all-gather.5.cloned.1.call-done = bf16[2048,256]{1,0:T(8,128)(2,1)} async-done(((bf16[256,256]{1,0:T(8,128)(2,1)}), bf16[2048,256]{1,0:T(8,128)(2,1)}) %all-gather.5.cloned.1.call-update) | async-done | bytes 1048592 | tf_op jit(solution)/shard_map/all_gather | solution.py:19
  129.1 2.3 %copy.41 = bf16[2048,256]{0,1:T(8,128)(2,1)} copy(bf16[2048,256]{1,0:T(8,128)(2,1)} %all-gather.5.cloned.1.call-done) | data formatting | bytes 2097152 | tf_op jit(solution)/shard_map/all_gather | solution.py:19
  131.3 1.8 fusion
  133.1 2.5 %fusion.1 = f32[2,2,256]{2,1,0:T(2,128)S(1)} fusion(f32[2,2,256,2048]{3,2,1,0:T(8,128)S(1)} %get-tuple-element.3, f32[2,2,256]{2,1,0:T(2,128)S(1)} %broadcast_maximum_fusion, pred[256,2048]{1,0:T(8,128)(4,1)S(1)} %iota_compare_fusion), kind=kLoop, calls=%fused_computation.3 | loop fusion | flops 10484736 | bytes 8921088 | tf_op jit(solution)/shard_map/reduce_sum | solution.py:31
  135.6 0.0 copy-start.4
  135.6 0.0 copy-start.5
  135.6 2.2 %fusion.20 = f32[2,2,256,128]{2,3,1,0:T(8,128)S(1)} fusion(bf16[2048,2,128,1]{0,2,3,1:T(8,128)(2,1)S(1)} %bitcast.71, f32[2,2,256,2048]{3,2,1,0:T(8,128)S(1)} %get-tuple-element.3, f32[2,2,256]{2,1,0:T(2,128)S(1)} %broadcast_maximum_fusion, pred[256,2048]{1,0:T(8,128)(4,1)S(1)} %iota_compare_fusion, f32[2,2,256]{2,1,0:T(2,128)S(1)} %fusion.1), kind=kOutput, calls=%fused_computation.24 | convolution fusion | flops 547487744 | bytes 10493952 | tf_op jit(solution)/shard_map/hmqk,khd->hmqd/dot_general | solution.py:32
  137.9 0.0 copy-done.4
  137.9 0.0 copy-start.3
  137.9 0.1 multiply_reduce_fusion
  138.1 0.1 multiply_convert_fusion.1
  138.2 0.0 copy-done
  138.2 1.5 convolution_convert_fusion.1
  139.6 0.0 reduce-scatter.3.cloned.1.call-update
  139.7 8.8 %reduce-scatter.5.cloned.1.call-done = bf16[640,512]{1,0:T(8,128)(2,1)} async-done(((bf16[640,2048]{1,0:T(8,128)(2,1)}), bf16[640,512]{1,0:T(8,128)(2,1)}) %reduce-scatter.5.cloned.1.call-update) | async-done | bytes 655376 | tf_op jit(solution)/shard_map/reduce_scatter | solution.py:90
  148.5 5.5 %all-to-all-start.1 = ((bf16[8,80,512]{2,1,0:T(8,128)(2,1)}), bf16[8,80,512]{2,1,0:T(8,128)(2,1)S(1)}, u32[]{:S(2)}, u32[]{:S(2)}) async-start(bf16[8,80,512]{2,1,0:T(8,128)(2,1)} %bitcast.72), calls=%async_computation.3 | async-start | bytes 1310720 | tf_op jit(solution)/shard_map/all_to_all | solution.py:94
  154.0 0.2 select_reduce_fusion
  154.2 16.9 %all-to-all-done.1 = bf16[8,80,512]{2,1,0:T(8,128)(2,1)S(1)} async-done(((bf16[8,80,512]{2,1,0:T(8,128)(2,1)}), bf16[8,80,512]{2,1,0:T(8,128)(2,1)S(1)}, u32[]{:S(2)}, u32[]{:S(2)}) %all-to-all-start.1) | async-done | bytes 655392 | tf_op jit(solution)/shard_map/all_to_all | solution.py:94
  171.1 1.3 convolution_convert_fusion.2
  172.4 3.9 %reduce-scatter.3.cloned.1.call-done = bf16[64,2048]{1,0:T(8,128)(2,1)} async-done(((bf16[256,2048]{1,0:T(8,128)(2,1)}), bf16[64,2048]{1,0:T(8,128)(2,1)}) %reduce-scatter.3.cloned.1.call-update) | async-done | bytes 262160 | tf_op jit(solution)/shard_map/reduce_scatter | solution.py:45
  (12 shorter events, 0.1 us)
Async XLA Ops:
  8.0 130.2 %copy-start = (bf16[256,2048]{1,0:T(8,128)(2,1)S(1)}, bf16[256,2048]{1,0:T(8,128)(2,1)}, u32[]{:S(2)}) copy-start(bf16[256,2048]{1,0:T(8,128)(2,1)} %param.18) | copy-start | bytes 3145732
  16.5 79.5 %all-to-all-start = ((bf16[8,80,2048]{2,1,0:T(8,128)(2,1)}), bf16[8,80,2048]{2,1,0:T(8,128)(2,1)}, u32[]{:S(2)}, u32[]{:S(2)}) async-start(bf16[8,80,2048]{2,1,0:T(8,128)(2,1)} %bitcast.68), calls=%async_computation.1 | async-start | bytes 5242880 | tf_op jit(solution)/shard_map/all_to_all | solution.py:79
  23.8 92.0 %all-gather.3.cloned.1.call-start = ((), (), s32[]{:S(2)}) async-start(), calls=%async_computation.4 | async-start | bytes 1179648 | tf_op jit(solution)/shard_map/all_gather | solution.py:18
  24.5 104.6 %all-gather.5.cloned.1.call-start = ((), (), s32[]{:S(2)}) async-start(), calls=%async_computation.5 | async-start | bytes 1179648 | tf_op jit(solution)/shard_map/all_gather | solution.py:19
  25.3 123.2 %reduce-scatter.5.cloned.1.call-start = ((), (), s32[]{:S(2)}) async-start(), calls=%async_computation.7 | async-start | bytes 3276800 | tf_op jit(solution)/shard_map/reduce_scatter | solution.py:90
  103.2 12.1 %copy-start.2 = (bf16[256,256]{1,0:T(8,128)(2,1)S(1)}, bf16[256,256]{1,0:T(8,128)(2,1)}, u32[]{:S(2)}) copy-start(bf16[256,256]{1,0:T(8,128)(2,1)} %param.13) | copy-start | bytes 393220
  115.0 61.2 %reduce-scatter.3.cloned.1.call-start = ((), (), s32[]{:S(2)}) async-start(), calls=%async_computation.6 | async-start | bytes 1310720 | tf_op jit(solution)/shard_map/reduce_scatter | solution.py:45
  133.1 2.5 %copy-start.1 = (bf16[2048,256]{0,1:T(8,128)(2,1)S(1)}, bf16[2048,256]{0,1:T(8,128)(2,1)}, u32[]{:S(2)}) copy-start(bf16[2048,256]{0,1:T(8,128)(2,1)} %copy.41) | copy-start | bytes 3145732
  135.6 2.3 %copy-start.4 = (f32[2]{0:T(128)S(1)}, f32[2]{0:T(128)}, u32[]{:S(2)}) copy-start(f32[2]{0:T(128)} %param.16) | copy-start | bytes 28
  135.6 2.4 %copy-start.5 = (f32[128]{0:T(128)S(1)}, f32[128]{0:T(128)}, u32[]{:S(2)}) copy-start(f32[128]{0:T(128)} %param.17) | copy-start | bytes 1540
  137.9 16.1 %copy-start.3 = (f32[192,2]{0,1:T(2,128)S(1)}, f32[192,2]{0,1:T(2,128)}, u32[]{:S(2)}) copy-start(f32[192,2]{0,1:T(2,128)} %param.22) | copy-start | bytes 4612
  148.5 22.6 %all-to-all-start.1 = ((bf16[8,80,512]{2,1,0:T(8,128)(2,1)}), bf16[8,80,512]{2,1,0:T(8,128)(2,1)S(1)}, u32[]{:S(2)}, u32[]{:S(2)}) async-start(bf16[8,80,512]{2,1,0:T(8,128)(2,1)} %bitcast.72), calls=%async_computation.3 | async-start | bytes 1310720 | tf_op jit(solution)/shard_map/all_to_all | solution.py:94
Sparse Core Ops, SparseCore 0:
  26.7 60.7 all-gather.2
  89.7 39.3 all-gather.4
Sparse Core Ops, SparseCore 1:
  115.1 33.3 reduce-scatter.4
  151.5 24.7 reduce-scatter.2
where the time goes:
time: 184 us
  waiting for transfers between devices  113 us (61%)
  matrix products  29.4 us (16%)
  between operations  15.7 us (9%)
  starting transfers between devices  13.2 us (7%)
  other arithmetic  6.48 us (4%)
  local copies, waits for them, and re-layouts  5.48 us (3%)
    all_to_all x1, waiting for transfers between devices, expert_half(): lax.all_to_all(outgoing.reshape(experts, capacity, model_width), 'ep', sp...  70.7 us
    all_to_all x1, waiting for transfers between devices, expert_half(): lax.all_to_all(summed.reshape(experts, capacity, col_count), 'ep', split_...  16.9 us
    dot_general x1, matrix products, expert_half(): jnp.dot(hidden, down_mat, preferred_element_type=jnp.float32)  11.8 us
    all_gather x1, waiting for transfers between devices, mixer_half(): value_piece = lax.all_gather(value_rows, 'ep', axis=0, tiled=True)  11.8 us
    reduce_scatter x1, waiting for transfers between devices, expert_half(): lax.psum_scatter(partial_result.astype(jnp.bfloat16), 'tp', scatter_dimen...  8.83 us
    all_to_all x1, starting transfers between devices, expert_half(): lax.all_to_all(outgoing.reshape(experts, capacity, model_width), 'ep', sp...  7.28 us
    dot_general x1, matrix products, expert_half(): gate_act = jnp.dot(arrived, gate_mat, preferred_element_type=jnp.float32)  7.18 us
    all_to_all x1, starting transfers between devices, expert_half(): lax.all_to_all(summed.reshape(experts, capacity, col_count), 'ep', split_...  5.54 us
  transfers between devices with their start and end apart: 6, of which 5 were waited for; matrix products, arithmetic and copies ran while one was open for 18% of the time, Pallas kernels for 0%

commit v1 on v0

v1 whole, which is shorter than its diff:
```python
import functools

import jax
import jax.numpy as jnp
from jax import lax
from jax.experimental import pallas as pl
from jax.experimental.pallas import tpu as pltpu
from jax.sharding import PartitionSpec as P

EPS = 1e-06
MESH = pl.DeviceIdType.MESH
F32 = jnp.float32
BF16 = jnp.bfloat16


def flip(index, bits):
    low = 1
    while low <= bits:
        if bits & low:
            index = index + low - 2 * low * ((index // low) % 2)
        low *= 2
    return index


def dot(a, b, dims=((1,), (0,)), precision=None):
    return lax.dot_general(a, b, (dims, ((), ())), precision=precision, preferred_element_type=F32)


def kernel(
    n_ep, cap, lam, q, k, v, gain, x, norm_gain, ids, route_w, wo_hbm, wg_hbm, wu_hbm, wd_hbm,
    mixer, expert,
    wo, wg, wu, wd, arr, hidden, part, sib, ysend, yrecv, res, ret, kbuf, vbuf,
    outb, qs, comb, acc, top, tot, att, hp, hsib, hysend, hyrecv,
    w_sem, d_send, d_recv, f_send, f_recv, r_send, r_recv, s_send, s_recv, y_send, y_recv,
    kv_send, kv_recv, h_send, h_recv,
):
    me = lax.axis_index("ep")
    tp = lax.axis_index("tp")
    half = n_ep // 2
    tokens, width = x.shape
    cols = width // 4
    units = wg.shape[1]
    core = tp % 2
    sib_tp, y_tp = flip(tp, 1), flip(tp, 2)

    def remote(src, dst, ssem, rsem, where):
        return pltpu.make_async_remote_copy(
            src_ref=src, dst_ref=dst, send_sem=ssem, recv_sem=rsem,
            device_id=where, device_id_type=MESH,
        )

    weights = [
        pltpu.make_async_copy(a, b, w_sem.at[i])
        for i, (a, b) in enumerate(((wg_hbm, wg), (wu_hbm, wu), (wd_hbm, wd), (wo_hbm, wo)))
    ]
    for copy in weights:
        copy.start()

    barrier = pltpu.get_barrier_semaphore()
    for d in range(1, n_ep):
        pl.semaphore_signal(barrier, inc=1, device_id=(flip(me, d), tp), device_id_type=MESH)
    for d in range(1, 4):
        pl.semaphore_signal(barrier, inc=1, device_id=(me, flip(tp, d)), device_id_type=MESH)

    lane = lax.broadcasted_iota(jnp.int32, (tokens, 128), 1)
    id0, id1 = ids[:, 0:1], ids[:, 1:2]
    hot0, hot1 = (lane == id0).astype(F32), (lane == id1).astype(F32)
    earlier = (
        lax.broadcasted_iota(jnp.int32, (tokens, tokens), 1)
        < lax.broadcasted_iota(jnp.int32, (tokens, tokens), 0)
    ).astype(F32).astype(BF16)
    rank = dot(earlier, (hot0 + hot1).astype(BF16))
    pos0 = (id0 * cap).astype(F32) + jnp.sum(rank * hot0, axis=1, keepdims=True)
    pos1 = (id1 * cap).astype(F32) + jnp.sum(rank * hot1, axis=1, keepdims=True)
    packed = jnp.where(lane == 0, pos0, jnp.where(lane == 1, pos1, 0.0))
    pick = (
        lax.broadcasted_iota(jnp.int32, (8, 128), 0) == lax.broadcasted_iota(jnp.int32, (8, 128), 1)
    ).astype(F32)
    pos_rows = dot(pick, packed, ((1,), (1,)), lax.Precision.HIGHEST)
    row0 = (pos_rows[0:1] + 0.5).astype(jnp.int32)
    row1 = (pos_rows[1:2] + 0.5).astype(jnp.int32)
    slots = n_ep * cap
    slot = lax.broadcasted_iota(jnp.int32, (slots, tokens), 0)
    dispatch = ((slot == row0) | (slot == row1)).astype(F32).astype(BF16)
    wide = x[...].astype(F32)
    inv = lax.rsqrt(jnp.mean(wide * wide, axis=-1, keepdims=True) + EPS)
    mine = pl.ds(pl.multiple_of(tp * cols, cols), cols)
    normed = (x[:, mine].astype(F32) * inv * norm_gain[:, mine]).astype(BF16)
    outb[...] = dot(dispatch, normed).astype(BF16).reshape(n_ep, cap, cols)
    slot_c = lax.broadcasted_iota(jnp.int32, (tokens, slots), 1)
    comb[...] = jnp.where(slot_c == pos0.astype(jnp.int32), route_w[:, 0:1], 0.0) + jnp.where(
        slot_c == pos1.astype(jnp.int32), route_w[:, 1:2], 0.0
    )
    arr[tp, me] = outb[me]
    kbuf[me] = k[...]
    vbuf[me] = v[...]
    pl.semaphore_wait(barrier, n_ep - 1 + 3)

    sends = {}
    for d in range(1, n_ep):
        to = flip(me, d)
        sends[d] = remote(
            outb.at[to], arr.at[tp, me], d_send.at[d], d_recv.at[d], (to, tp)
        )
        sends[d].start()

    pending = [[], []]
    relays = [[], []]

    def forward(group):
        for d in range(group * half, (group + 1) * half):
            src = flip(me, d)
            if d:
                sends[d].wait_recv()
            for j, to in ((0, sib_tp), (1, y_tp)):
                c = remote(arr.at[tp, src], arr.at[tp, src], f_send.at[j, d], f_recv.at[j, d], (me, to))
                c.start()
                pending[group].append((j, c))

    def relay(group):
        first = [c for j, c in pending[group] if j == 1]
        for i, d in enumerate(range(group * half, (group + 1) * half)):
            first[i].wait_recv()
            src = flip(me, d)
            c = remote(
                arr.at[y_tp, src], arr.at[y_tp, src], f_send.at[2, d], f_recv.at[2, d], (me, sib_tp)
            )
            c.start()
            relays[group].append(c)

    def arrived(group):
        for j, c in pending[group]:
            if j == 0:
                c.wait_recv()
        for c in relays[group]:
            c.wait_recv()

    mine_half = me // half
    rows = half * cap

    def base_of(group):
        return (mine_half + group * (1 - 2 * mine_half)) * half

    def gate_up(group):
        base = base_of(group)

        def step(i, carry):
            at = pl.ds(pl.multiple_of(i * 128, 128), 128)
            total = jnp.zeros((rows, 256), F32)
            for t in range(4):
                w = jnp.concatenate(
                    [wg[t * cols:(t + 1) * cols, at], wu[t * cols:(t + 1) * cols, at]], axis=1
                )
                total += dot(arr[t, pl.ds(base, half)].reshape(rows, cols), w)
            g, u = total[:, :128], total[:, 128:]
            hidden[:, at] = (g / (1.0 + jnp.exp(-g)) * u).astype(BF16)
            return carry

        lax.fori_loop(0, units // 128, step, 0)

    def down(group):
        base = base_of(group)
        for t in range(4):
            def step(i, carry):
                at = pl.multiple_of(i * 256, 256)
                out = dot(hidden[...], wd[:, pl.ds(t * cols + at, 256)])
                part[t, pl.ds(base, half), :, pl.ds(at, 256)] = out.astype(BF16).reshape(half, cap, 256)
                return carry

            lax.fori_loop(0, cols // 256, step, 0)

    def pair_sum(group):
        base = base_of(group)
        copies = []
        for y in range(2):
            c = remote(
                part.at[2 * y + 1 - core, pl.ds(base, half)], sib.at[y, pl.ds(base, half)],
                s_send.at[group, y], s_recv.at[group, y], (me, sib_tp),
            )
            c.start()
            copies.append(c)
        return copies

    my_y = tp // 2

    def y_sum(group, copies):
        base = base_of(group)
        at = pl.ds(base, half)
        for c in copies:
            c.wait()
        ysend[at] = (part[y_tp, at].astype(F32) + sib[1 - my_y, at].astype(F32)).astype(BF16)
        c = remote(ysend.at[at], yrecv.at[at], y_send.at[group], y_recv.at[group], (me, y_tp))
        c.start()
        return c

    def give_back(group, copy):
        base = base_of(group)
        at = pl.ds(base, half)
        copy.wait()
        res[at] = (
            part[tp, at].astype(F32) + sib[my_y, at].astype(F32) + yrecv[at].astype(F32)
        ).astype(BF16)
        out = []
        for d in range(group * half, (group + 1) * half):
            if d:
                to = flip(me, d)
                c = remote(res.at[to], ret.at[me], r_send.at[d], r_recv.at[d], (to, tp))
                c.start()
                out.append(c)
            else:
                ret[me] = res[me]
        return out

    across = flip(me, 1)
    level, side = me // 2, me % 2
    levels = n_ep // 2

    def kv_copy(b, way, up):
        buf = kbuf if b == 0 else vbuf
        def make(block):
            to = lax.rem(me + 2, n_ep) if up else across
            idx = block // 2
            return remote(
                buf.at[block], buf.at[block], kv_send.at[way, b, idx], kv_recv.at[way, b, idx], (to, tp)
            )
        return make

    def kv_send_block(lev):
        block = 2 * lev + side

        @pl.when(level < levels - 1)
        def _():
            for b in range(2):
                kv_copy(b, 0, True)(block).start()

        @pl.when((lev < level) | (side == 0))
        def _():
            for b in range(2):
                kv_copy(b, 1, False)(block).start()

    def kv_hop(step):
        @pl.when(level - step >= 0)
        def _():
            lev = level - step
            for b in range(2):
                kv_copy(b, 0, True)(2 * lev + side).wait_recv()
            kv_send_block(lev)

    def kv_across(lev):
        block = 2 * lev + 1 - side
        for b in range(2):
            kv_copy(b, 1, False)(block).wait_recv()

    def kv_finish():
        def step(lev, carry):
            block = 2 * lev + side

            @pl.when(level < levels - 1)
            def _():
                for b in range(2):
                    kv_copy(b, 0, True)(block).wait_send()

            @pl.when((lev < level) | (side == 0))
            def _():
                for b in range(2):
                    kv_copy(b, 1, False)(block).wait_send()

            return carry

        lax.fori_loop(0, level + 1, step, 0)

    q_rows = q.shape[0]
    heads = lam.shape[0]
    pair = q.shape[1] // heads
    head_width = pair // 2
    head_lane = lax.broadcasted_iota(jnp.int32, (q_rows, pair), 1)

    def attend_own():
        for h in range(heads):
            at = slice(h * pair, (h + 1) * pair)
            qh = q[:, at].astype(F32) * (head_width ** -0.5)
            qs[h, :q_rows] = jnp.where(head_lane < head_width, qh, 0.0).astype(BF16)
            qs[h, q_rows:] = jnp.where(head_lane < head_width, 0.0, qh).astype(BF16)
            s = dot(qs[h], k[:, at], ((1,), (1,)))
            qp = lax.broadcasted_iota(jnp.int32, s.shape, 0) % q_rows
            ok = qp >= lax.broadcasted_iota(jnp.int32, s.shape, 1)
            s = jnp.where(ok, s, -1e30)
            m = jnp.max(s, axis=1, keepdims=True)
            w = jnp.where(ok, jnp.exp(s - m), 0.0)
            top[h] = m
            tot[h] = jnp.sum(w, axis=1, keepdims=True)
            acc[h] = dot(w.astype(BF16), v[:, at])

    def attend(block):
        kb, vb = kbuf.at[block], vbuf.at[block]
        for h in range(heads):
            at = slice(h * pair, (h + 1) * pair)
            s = dot(qs[h], kb[:, at], ((1,), (1,)))
            old = top[h]
            m = jnp.maximum(old, jnp.max(s, axis=1, keepdims=True))
            scale = jnp.exp(old - m)
            w = jnp.exp(s - m)
            top[h] = m
            tot[h] = tot[h] * scale + jnp.sum(w, axis=1, keepdims=True)
            acc[h] = acc[h] * scale + dot(w.astype(BF16), vb[:, at])

    def attend_rest():
        def step(i, carry):
            lev = level - i

            @pl.when(i > 0)
            def _():
                attend(2 * lev + side)

            @pl.when((i > 0) | (side == 1))
            def _():
                kv_across(lev)
                attend(2 * lev + 1 - side)

            return carry

        lax.fori_loop(0, level + 1, step, 0)

    def project():
        outs = []
        for h in range(heads):
            a = acc[h] / tot[h]
            contrast = a[:q_rows] - lam[h] * a[q_rows:]
            norm = lax.rsqrt(jnp.mean(contrast * contrast, axis=-1, keepdims=True) + EPS)
            outs.append((contrast * norm * gain[...]).astype(BF16))
        att[...] = jnp.concatenate(outs, axis=1)

        def step(i, carry):
            at = pl.ds(pl.multiple_of(i * 256, 256), 256)
            hp[:, :, at] = dot(att[...], wo[:, at]).astype(BF16).reshape(4, q_rows // 4, 256)
            return carry

        lax.fori_loop(0, width // 256, step, 0)
        copies = []
        for y in range(2):
            c = remote(
                hp.at[2 * y + 1 - core], hsib.at[y], h_send.at[y], h_recv.at[y], (me, sib_tp)
            )
            c.start()
            copies.append(c)
        return copies

    forward(0)
    relay(0)
    forward(1)
    kv_send_block(level)
    weights[0].wait()
    weights[1].wait()
    arrived(0)
    gate_up(0)
    relay(1)
    weights[2].wait()
    down(0)
    pair0 = pair_sum(0)
    kv_hop(1)
    arrived(1)
    gate_up(1)
    y0 = y_sum(0, pair0)
    for step in range(2, min(levels, 3)):
        kv_hop(step)
    down(1)
    pair1 = pair_sum(1)
    for step in range(3, levels):
        kv_hop(step)
    attend_own()
    back = give_back(0, y0)
    y1 = y_sum(1, pair1)
    attend_rest()
    back += give_back(1, y1)
    weights[3].wait()
    hcopies = project()
    for c in hcopies:
        c.wait()
    hysend[...] = (hp[y_tp].astype(F32) + hsib[1 - my_y].astype(F32)).astype(BF16)
    hy = remote(hysend, hyrecv, h_send.at[2], h_recv.at[2], (me, y_tp))
    hy.start()
    for d in range(1, n_ep):
        sends[d].wait_send()
    for group in range(2):
        for j, c in pending[group]:
            c.wait_send()
        for c in relays[group]:
            c.wait_send()
    kv_finish()
    hy.wait()
    mixer[...] = (hp[tp].astype(F32) + hsib[my_y].astype(F32) + hyrecv[...].astype(F32)).astype(BF16)
    for c in back:
        c.wait()
    big = comb[...]
    high = big.astype(BF16)
    low = (big - high.astype(F32)).astype(BF16)
    got = ret[...].reshape(slots, cols)
    expert[...] = (dot(high, got) + dot(low, got)).astype(BF16)


def solution(mesh):
    n_ep = mesh.shape["ep"]

    def shards(
        queries, key_rows, value_rows, head_lambda, sub_gain, out_weight, expert_input, norm_gain,
        route_ids, route_weight, gate_weight, up_weight, down_weight,
    ):
        tokens, width = expert_input.shape
        cap = 5 * route_ids.shape[1] * tokens // (3 * n_ep)
        cap = -(-cap // 16) * 16
        cols = width // 4
        half = n_ep // 2
        units = gate_weight.shape[2]
        q_rows, kv_cols = queries.shape
        heads = head_lambda.shape[0]
        vm = pl.BlockSpec(memory_space=pltpu.VMEM)
        hbm = pl.BlockSpec(memory_space=pl.ANY)
        dma = pltpu.SemaphoreType.DMA
        return pl.pallas_call(
            functools.partial(kernel, n_ep, cap),
            name="both_halves",
            out_shape=(
                jax.ShapeDtypeStruct((q_rows // 4, width), BF16),
                jax.ShapeDtypeStruct((tokens, cols), BF16),
            ),
            in_specs=[pl.BlockSpec(memory_space=pltpu.SMEM)] + [vm] * 8 + [hbm] * 4,
            out_specs=(vm, vm),
            scratch_shapes=[
                pltpu.VMEM(out_weight.shape, BF16),
                pltpu.VMEM((width, units), BF16),
                pltpu.VMEM((width, units), BF16),
                pltpu.VMEM((units, width), BF16),
                pltpu.VMEM((4, n_ep, cap, cols), BF16),
                pltpu.VMEM((half * cap, units), BF16),
                pltpu.VMEM((4, n_ep, cap, cols), BF16),
                pltpu.VMEM((2, n_ep, cap, cols), BF16),
                pltpu.VMEM((n_ep, cap, cols), BF16),
                pltpu.VMEM((n_ep, cap, cols), BF16),
                pltpu.VMEM((n_ep, cap, cols), BF16),
                pltpu.VMEM((n_ep, cap, cols), BF16),
                pltpu.VMEM((n_ep, q_rows, kv_cols), BF16),
                pltpu.VMEM((n_ep, q_rows, kv_cols), BF16),
                pltpu.VMEM((n_ep, cap, cols), BF16),
                pltpu.VMEM((heads, 2 * q_rows, 128), BF16),
                pltpu.VMEM((tokens, n_ep * cap), F32),
                pltpu.VMEM((heads, 2 * q_rows, 128), F32),
                pltpu.VMEM((heads, 2 * q_rows, 1), F32),
                pltpu.VMEM((heads, 2 * q_rows, 1), F32),
                pltpu.VMEM((q_rows, kv_cols), BF16),
                pltpu.VMEM((4, q_rows // 4, width), BF16),
                pltpu.VMEM((2, q_rows // 4, width), BF16),
                pltpu.VMEM((q_rows // 4, width), BF16),
                pltpu.VMEM((q_rows // 4, width), BF16),
                dma((4,)),
                dma((n_ep,)), dma((n_ep,)),
                dma((3, n_ep)), dma((3, n_ep)),
                dma((n_ep,)), dma((n_ep,)),
                dma((2, 2)), dma((2, 2)),
                dma((2,)), dma((2,)),
                dma((2, 2, half)), dma((2, 2, half)),
                dma((3,)), dma((3,)),
            ],
            compiler_params=pltpu.CompilerParams(
                collective_id=0, has_side_effects=True, vmem_limit_bytes=62 * 1024 * 1024
            ),
        )(
            head_lambda, queries, key_rows, value_rows, sub_gain.reshape(1, -1), expert_input,
            norm_gain.reshape(1, -1), route_ids, route_weight, out_weight,
            gate_weight[0], up_weight[0], down_weight[0],
        )

    placed = (
        P("ep", "tp"), P("ep", "tp"), P("ep", "tp"), P("tp"), P(), P("tp", None), P("ep", None), P(),
        P("ep", None), P("ep", None), P("ep", None, "tp"), P("ep", None, "tp"), P("ep", "tp", None),
    )
    return jax.shard_map(
        shards, mesh=mesh, in_specs=placed,
        out_specs=(P(("ep", "tp"), None), P("ep", "tp")), check_vma=False,
    )
```

time: 184 us -> 77.1 us (0.42)
  waiting for transfers between devices: 113 us -> 0 us
  Pallas kernels: 0 us -> 70 us
  matrix products: 29.4 us -> 0 us
  between operations: 15.7 us -> 0.64 us
  starting transfers between devices: 13.2 us -> 0 us
  other arithmetic: 6.48 us -> 0 us
    all_to_all x2 -> x0, waiting for transfers between devices: 87.6 us -> none  [the longest x1 70.7 us: expert_half(): lax.all_to_all(outgoing.reshape(experts, capacity, model_width), 'ep', sp...]
    pallas_call x0 -> x1, Pallas kernels: none -> 70 us  [shards(): pl.pallas_call(functools.partial(kernel, n_ep, cap), name='both_halves',...]
    dot_general x7 -> x0, matrix products: 29.4 us -> none  [the longest x1 11.8 us: expert_half(): jnp.dot(hidden, down_mat, preferred_element_type=jnp.float32)]
    all_to_all x2 -> x0, starting transfers between devices: 12.8 us -> none  [the longest x1 7.28 us: expert_half(): lax.all_to_all(outgoing.reshape(experts, capacity, model_width), 'ep', sp...]
    reduce_scatter x2 -> x0, waiting for transfers between devices: 12.7 us -> none  [the longest x1 8.83 us: expert_half(): lax.psum_scatter(partial_result.astype(jnp.bfloat16), 'tp', scatter_dimen...]
    all_gather x2 -> x0, waiting for transfers between devices: 11.8 us -> none  [the longest x1 11.8 us: mixer_half(): value_piece = lax.all_gather(value_rows, 'ep', axis=0, tiled=True)]
    unnamed x14 -> x4, local copies, waits for them, and re-layouts: 1.02 us -> 6.17 us
    reduce_sum x5 -> x0, other arithmetic: 4.22 us -> none  [the longest x1 2.46 us: mixer_half(): row_total = jnp.sum(weights, axis=-1)]
  transfers between devices with their start and end apart: 6 -> 0, of which waited for: 5 -> 0; matrix products, arithmetic and copies ran while one was open for 18% -> 0% of each run, Pallas kernels for 0% -> 0%
where the time goes in v1:
time: 77.1 us; the launch traced here: 76.8 us
  Pallas kernels  70 us (91%)
  local copies, waits for them, and re-layouts  6.17 us (8%)
    pallas_call x1, Pallas kernels, shards(): pl.pallas_call(functools.partial(kernel, n_ep, cap), name='both_halves',...  70 us
    unnamed x4, local copies, waits for them, and re-layouts  6.17 us

profile of v1, /device:TPU:0, one launch (start us, length us, event | category | flops | bytes accessed | tf_op | source)
XLA Modules:
  0.0 76.8 jit_solution(7315169039405915541)
XLA Ops:
  0.6 1.4 %copy.15.ids = s32[192,2]{1,0:T(8,128)} copy(s32[192,2]{0,1:T(2,128)} %param.21) | data formatting | bytes 3072 | tf_op args[8]
  2.1 1.4 %copy.16.route_w = f32[192,2]{1,0:T(8,128)} copy(f32[192,2]{0,1:T(2,128)} %param.22) | data formatting | bytes 3072 | tf_op args[9]
  3.5 70.0 %both_halves.1 = (bf16[64,2048]{1,0:T(8,128)(2,1)}, bf16[192,512]{1,0:T(8,128)(2,1)}) custom-call(f32[2]{0:T(128)} %lam.1, bf16[256,256]{1,0:T(8,128)(2,1)} %q.1, bf16[256,256]{1,0:T(8,128)(2,1)} %k.1, bf16[256,256]{1,0:T(8,128)(2,1)} %v.1, f32[1,128]{1,0:T(1,128)} %bitcast.9, bf16[192,2048]{1,0:T(8,128)(2,1)} %x.1, f32[1,2048]{1,0:T(1,128)} %bitcast.8, ...), custom_call_target="tpu_custom_call" | custom-call | tf_op jit(solution)/shard_map/both_halves/pallas_call | solution.py:419
  73.5 1.7 %copy.19 = bf16[64,2048]{1,0:T(8,128)(2,1)} copy(bf16[64,2048]{1,0:T(8,128)(2,1)} %get-tuple-element.4) | data formatting | bytes 524288
  75.2 1.6 %copy.20 = bf16[192,512]{1,0:T(8,128)(2,1)} copy(bf16[192,512]{1,0:T(8,128)(2,1)} %get-tuple-element.5) | data formatting | bytes 393216

commit v2 on v1

--- a/solution.py
+++ b/solution.py
@@ -30,7 +30,7 @@
     n_ep, cap, lam, q, k, v, gain, x, norm_gain, ids, route_w, wo_hbm, wg_hbm, wu_hbm, wd_hbm,
     mixer, expert,
     wo, wg, wu, wd, arr, hidden, part, sib, ysend, yrecv, res, ret, kbuf, vbuf,
-    outb, qs, comb, acc, top, tot, att, hp, hsib, hysend, hyrecv,
+    outb, qs, comb, acc, top, att, hp, hsib, hysend, hyrecv,
     w_sem, d_send, d_recv, f_send, f_recv, r_send, r_recv, s_send, s_recv, y_send, y_recv,
     kv_send, kv_recv, h_send, h_recv,
 ):
@@ -225,13 +225,16 @@
             )
         return make
 
-    def kv_send_block(lev):
+    def kv_up(lev):
         block = 2 * lev + side
 
         @pl.when(level < levels - 1)
         def _():
             for b in range(2):
                 kv_copy(b, 0, True)(block).start()
+
+    def kv_over(lev):
+        block = 2 * lev + side
 
         @pl.when((lev < level) | (side == 0))
         def _():
@@ -244,7 +247,8 @@
             lev = level - step
             for b in range(2):
                 kv_copy(b, 0, True)(2 * lev + side).wait_recv()
-            kv_send_block(lev)
+            kv_up(lev)
+            kv_over(lev)
 
     def kv_across(lev):
         block = 2 * lev + 1 - side
@@ -288,43 +292,42 @@
             m = jnp.max(s, axis=1, keepdims=True)
             w = jnp.where(ok, jnp.exp(s - m), 0.0)
             top[h] = m
-            tot[h] = jnp.sum(w, axis=1, keepdims=True)
-            acc[h] = dot(w.astype(BF16), v[:, at])
-
-    def attend(block):
-        kb, vb = kbuf.at[block], vbuf.at[block]
+            acc[h] = dot(w.astype(BF16), with_ones(v[:, at]))
+
+    def with_ones(vb):
+        return jnp.concatenate([vb, jnp.ones(vb.shape, BF16)], axis=1)
+
+    def attend(first, count):
+        span = pl.ds(first, count)
         for h in range(heads):
             at = slice(h * pair, (h + 1) * pair)
-            s = dot(qs[h], kb[:, at], ((1,), (1,)))
+            kb = kbuf[span, :, at].reshape(count * q_rows, pair)
+            vb = vbuf[span, :, at].reshape(count * q_rows, pair)
+            s = dot(qs[h], kb, ((1,), (1,)))
             old = top[h]
             m = jnp.maximum(old, jnp.max(s, axis=1, keepdims=True))
-            scale = jnp.exp(old - m)
             w = jnp.exp(s - m)
             top[h] = m
-            tot[h] = tot[h] * scale + jnp.sum(w, axis=1, keepdims=True)
-            acc[h] = acc[h] * scale + dot(w.astype(BF16), vb[:, at])
-
-    def attend_rest():
+            acc[h] = acc[h] * jnp.exp(old - m) + dot(w.astype(BF16), with_ones(vb))
+
+    def attend_level():
+        @pl.when(side == 1)
+        def _():
+            kv_across(level)
+            attend(2 * level, 1)
+
+    def attend_rest(lo, hi):
         def step(i, carry):
-            lev = level - i
-
-            @pl.when(i > 0)
-            def _():
-                attend(2 * lev + side)
-
-            @pl.when((i > 0) | (side == 1))
-            def _():
-                kv_across(lev)
-                attend(2 * lev + 1 - side)
-
+            kv_across(level - i)
+            attend(2 * (level - i), 2)
             return carry
 
-        lax.fori_loop(0, level + 1, step, 0)
+        lax.fori_loop(lo, jnp.minimum(hi, level + 1), step, 0)
 
     def project():
         outs = []
         for h in range(heads):
-            a = acc[h] / tot[h]
+            a = acc[h, :, :pair] / acc[h, :, pair:]
             contrast = a[:q_rows] - lam[h] * a[q_rows:]
             norm = lax.rsqrt(jnp.mean(contrast * contrast, axis=-1, keepdims=True) + EPS)
             outs.append((contrast * norm * gain[...]).astype(BF16))
@@ -345,10 +348,12 @@
             copies.append(c)
         return copies
 
+    kv_over(level)
+    attend_own()
     forward(0)
     relay(0)
     forward(1)
-    kv_send_block(level)
+    kv_up(level)
     weights[0].wait()
     weights[1].wait()
     arrived(0)
@@ -367,11 +372,12 @@
     pair1 = pair_sum(1)
     for step in range(3, levels):
         kv_hop(step)
-    attend_own()
     back = give_back(0, y0)
+    attend_level()
     y1 = y_sum(1, pair1)
-    attend_rest()
+    attend_rest(1, 2)
     back += give_back(1, y1)
+    attend_rest(2, levels)
     weights[3].wait()
     hcopies = project()
     for c in hcopies:
@@ -443,8 +449,7 @@
                 pltpu.VMEM((n_ep, cap, cols), BF16),
                 pltpu.VMEM((heads, 2 * q_rows, 128), BF16),
                 pltpu.VMEM((tokens, n_ep * cap), F32),
-                pltpu.VMEM((heads, 2 * q_rows, 128), F32),
-                pltpu.VMEM((heads, 2 * q_rows, 1), F32),
+                pltpu.VMEM((heads, 2 * q_rows, 2 * kv_cols // heads), F32),
                 pltpu.VMEM((heads, 2 * q_rows, 1), F32),
                 pltpu.VMEM((q_rows, kv_cols), BF16),
                 pltpu.VMEM((4, q_rows // 4, width), BF16),

time: 77.1 us -> 72.3 us (0.938)
  Pallas kernels: 70 us -> 64.8 us
    pallas_call x1, Pallas kernels: 70 us -> 64.8 us  [shards(): pl.pallas_call(functools.partial(kernel, n_ep, cap), name='both_halves',...]
where the time goes in v2:
time: 72.3 us; the launch traced here: 71.6 us
  Pallas kernels  64.8 us (90%)
  local copies, waits for them, and re-layouts  6.17 us (9%)
    pallas_call x1, Pallas kernels, shards(): pl.pallas_call(functools.partial(kernel, n_ep, cap), name='both_halves',...  64.8 us
    unnamed x4, local copies, waits for them, and re-layouts  6.17 us

profile of v2, /device:TPU:0, one launch (start us, length us, event | category | flops | bytes accessed | tf_op | source)
XLA Modules:
  0.0 71.6 jit_solution(10306454347401243258)
XLA Ops:
  0.6 1.4 %copy.15.ids = s32[192,2]{1,0:T(8,128)} copy(s32[192,2]{0,1:T(2,128)} %param.21) | data formatting | bytes 3072 | tf_op args[8]
  2.1 1.4 %copy.16.route_w = f32[192,2]{1,0:T(8,128)} copy(f32[192,2]{0,1:T(2,128)} %param.22) | data formatting | bytes 3072 | tf_op args[9]
  3.5 64.8 %both_halves.1 = (bf16[64,2048]{1,0:T(8,128)(2,1)}, bf16[192,512]{1,0:T(8,128)(2,1)}) custom-call(f32[2]{0:T(128)} %lam.1, bf16[256,256]{1,0:T(8,128)(2,1)} %q.1, bf16[256,256]{1,0:T(8,128)(2,1)} %k.1, bf16[256,256]{1,0:T(8,128)(2,1)} %v.1, f32[1,128]{1,0:T(1,128)} %bitcast.9, bf16[192,2048]{1,0:T(8,128)(2,1)} %x.1, f32[1,2048]{1,0:T(1,128)} %bitcast.8, ...), custom_call_target="tpu_custom_call" | custom-call | tf_op jit(solution)/shard_map/both_halves/pallas_call | solution.py:425
  68.3 1.7 %copy.19 = bf16[64,2048]{1,0:T(8,128)(2,1)} copy(bf16[64,2048]{1,0:T(8,128)(2,1)} %get-tuple-element.4) | data formatting | bytes 524288
  69.9 1.6 %copy.20 = bf16[192,512]{1,0:T(8,128)(2,1)} copy(bf16[192,512]{1,0:T(8,128)(2,1)} %get-tuple-element.5) | data formatting | bytes 393216
